TPU v7x, 32 devices: a whole 2x2x4 slice. The times are simulated.
32 devices in a mesh: ep: 8 (over z, x), tp: 4 (over y, core).
Axes of the slice: x: 2, y: 2, z: 4, core: 2. Of those that a mesh axis runs over, the one named last changes fastest.
Arguments:
- tokens: bfloat16 [2048, 4096], P('ep', 'tp'), may hold values from -72 to 72
- pre_gain: float32 [4096], P('tp'), may hold values from 0.1 to 1.9
- expert_ids: int32 [2048, 3], P('ep'), may hold values from 0 to 15, all different within a row; in each aligned block of 256 rows (0 to 255, 256 to 511, ...) at most 64 rows name the same one
- route_weight: float32 [2048, 3], P('ep'), may hold values from 0.2 to 2
- expert_gate: bfloat16 [16, 1024, 4096], P('ep', 'tp'), may hold values from -0.09375 to 0.09375
- expert_up: bfloat16 [16, 1024, 4096], P('ep', 'tp'), may hold values from -0.09375 to 0.09375
- expert_down: bfloat16 [16, 1024, 4096], P('ep', None, 'tp'), may hold values from -0.9375 to 0.9375
- shared_gate: bfloat16 [1024, 4096], P('tp'), may hold values from -0.09375 to 0.09375
- shared_up: bfloat16 [1024, 4096], P('tp'), may hold values from -0.09375 to 0.09375
- shared_down: bfloat16 [1024, 4096], P(None, 'tp'), may hold values from -0.9375 to 0.9375
- out_gain: float32 [4096], P('tp'), may hold values from 0.1 to 1.9
Outputs:
- mixed: bfloat16 [2048, 4096], P('ep', 'tp')
Inputs may be any that keep to these rules, and one draw needn't show every extreme that they name: `expert_ids`: A row names 3 different experts. Among the rows of one index of ep no expert is named more than 64 times, and in every draw some expert is named exactly 64 times there.
All inputs are finite; a program needn't handle non-finite values.
Results may differ from a plain program's by a relative error of at most 0.0068.
Values may be sent and summed in bfloat16 or wider, within the bound.
A program may use at most 64 MiB of HBM per device.

v0:
```python
import jax
import jax.numpy as jnp
from jax import lax
from jax.sharding import PartitionSpec as P

D = 4096


EPSILON = 1e-06


def expert_slots(flat_ids, experts, capacity):
    count = flat_ids.shape[0]
    one_hot = (flat_ids[:, None] == jnp.arange(experts, dtype=jnp.int32)[None, :]).astype(jnp.int32)
    before = jnp.cumsum(one_hot, axis=0) - one_hot
    slot_index = jnp.sum(before * one_hot, axis=1)
    dest_index = flat_ids * capacity + slot_index
    source = (
        jnp.full((experts * capacity,), -1, jnp.int32)
        .at[dest_index]
        .set(jnp.arange(count, dtype=jnp.int32))
    )
    return (dest_index, source)


def on_device(
    tokens,
    pre_gain,
    expert_ids,
    route_weight,
    expert_gate,
    expert_up,
    expert_down,
    shared_gate,
    shared_up,
    shared_down,
    out_gain,
):
    tok_count, top_count = expert_ids.shape
    exp_dev = expert_gate.shape[0]
    n_ep = lax.axis_size("ep")
    experts = exp_dev * n_ep
    capacity = 4 * tok_count * top_count // (3 * experts)
    feat_local = tokens.shape[1]
    tok_float = tokens.astype(jnp.float32)
    square_sum = lax.psum(jnp.sum(tok_float * tok_float, axis=1), "tp")
    normed = (tok_float * lax.rsqrt(square_sum[:, None] / D + EPSILON) * pre_gain).astype(
        jnp.bfloat16
    )
    flat_ids = expert_ids.reshape(tok_count * top_count)
    dest_index, source = expert_slots(flat_ids, experts, capacity)
    is_live = (source >= 0)[:, None].astype(jnp.bfloat16)
    picked = jnp.where(source >= 0, source // top_count, 0)
    outgoing = (normed[picked] * is_live).reshape(experts, capacity, feat_local)
    arrived = lax.all_to_all(outgoing, "ep", split_axis=0, concat_axis=1, tiled=True)
    segment = lax.all_gather(arrived, "tp", axis=2, tiled=True)
    gate_piece = expert_gate
    up_piece = expert_up
    gate_next = jnp.einsum("esd,efd->esf", segment, gate_piece, preferred_element_type=jnp.float32)
    up_next = jnp.einsum("esd,efd->esf", segment, up_piece, preferred_element_type=jnp.float32)
    gate_sum = gate_next
    up_sum = up_next
    segment = lax.all_gather(normed, "tp", axis=1, tiled=True)
    gate_piece = shared_gate
    up_piece = shared_up
    gate_next = jnp.einsum("td,fd->tf", segment, gate_piece, preferred_element_type=jnp.float32)
    up_next = jnp.einsum("td,fd->tf", segment, up_piece, preferred_element_type=jnp.float32)
    hidden_act = (jax.nn.silu(gate_sum) * up_sum).astype(jnp.bfloat16)
    down_piece = expert_down
    expert_out = jnp.einsum(
        "esf,efd->esd",
        lax.all_gather(hidden_act, "tp", axis=2, tiled=True),
        down_piece,
        preferred_element_type=jnp.float32,
    ).astype(jnp.bfloat16)
    returned = lax.all_to_all(expert_out, "ep", split_axis=1, concat_axis=0, tiled=True).reshape(
        experts * capacity, feat_local
    )
    route_rows = returned[dest_index].reshape(tok_count, top_count, feat_local).astype(jnp.float32)
    routed = jnp.sum(route_rows * route_weight[:, :, None], axis=1)
    shared_act = (jax.nn.silu(gate_next) * up_next).astype(jnp.bfloat16)
    down_piece = shared_down
    shared_out = jnp.dot(
        lax.all_gather(shared_act, "tp", axis=1, tiled=True),
        down_piece,
        preferred_element_type=jnp.float32,
    )
    summed = routed + shared_out
    out_square = lax.psum(jnp.sum(summed * summed, axis=1), "tp")
    return (summed * lax.rsqrt(out_square[:, None] / D + EPSILON) * out_gain).astype(jnp.bfloat16)


def solution(mesh):
    return jax.shard_map(
        on_device,
        mesh=mesh,
        in_specs=(
            P("ep", "tp"),
            P("tp"),
            P("ep", None),
            P("ep", None),
            P("ep", "tp", None),
            P("ep", "tp", None),
            P("ep", None, "tp"),
            P("tp", None),
            P("tp", None),
            P(None, "tp"),
            P("tp"),
        ),
        out_specs=P("ep", "tp"),
        check_vma=False,
    )
```

profile of v0, /device:TPU:0, one launch (start us, length us, event | category | flops | bytes accessed | tf_op | source)
XLA Modules:
  0.0 276.5 jit_solution(14706495626162394263)
XLA Ops:
  6.5 1.0 copy.22
  7.9 0.7 broadcast_multiply_fusion.1
  8.6 1.7 reduce-window.6
  11.1 3.4 %scatter_custom_fusion = s32[1024]{0:T(1024)S(1)} fusion(s32[768]{0:T(1024)S(1)} %fusion.12, s32[768]{0:T(1024)S(1)} %iota.11, s32[]{:T(128)} %constant.17.clone.1), kind=kCustom, calls=%fused_computation.40 | custom fusion | bytes 4100 | tf_op jit(solution)/shard_map/scatter | solution.py:21
  14.5 1.2 fusion.2
  15.8 8.4 %psum.14 = f32[256]{0:T(256)S(1)} all-reduce(f32[256]{0:T(256)S(1)} %fusion.2), channel_id=1, replica_groups=mesh['ep'=8,'tp'=4] {'tp'}, use_global_device_ids=true, to_apply=%region_1.0 | all-reduce | flops 256 | bytes 2048 | tf_op jit(solution)/shard_map/psum | solution.py:46
  24.2 1.2 fusion.4
  25.5 5.4 %gather_fusion = bf16[1024,1024]{1,0:T(8,128)(2,1)} fusion(bf16[256,1024]{1,0:T(8,128)(2,1)S(1)} %fusion.4, s32[1024]{0:T(1024)S(1)} %fusion.10), kind=kCustom, calls=%fused_computation | custom fusion | bytes 4198400 | tf_op jit(solution)/shard_map/gather | solution.py:54
  30.9 1.8 broadcast_multiply_fusion
  32.7 52.6 %all_to_all.33 = bf16[16,64,1024]{2,1,0:T(8,128)(2,1)S(1)} all-to-all(bf16[16,64,1024]{2,1,0:T(8,128)(2,1)S(1)} %broadcast_multiply_fusion), channel_id=1, replica_groups=mesh['ep'=8,'tp'=4] {'ep'}, dimensions={0} | all-to-all | bytes 4194304 | tf_op jit(solution)/shard_map/all_to_all | solution.py:55
  85.3 1.6 copy.25
  87.0 57.4 %all-gather.4.cloned.1.call-done = bf16[2,512,4096]{2,1,0:T(8,128)(2,1)} async-done(((bf16[2,512,1024]{2,1,0:T(8,128)(2,1)}), bf16[2,512,4096]{2,1,0:T(8,128)(2,1)}) %all-gather.4.cloned.1.call-update) | async-done | bytes 8388624 | tf_op jit(solution)/shard_map/all_gather | solution.py:56
  144.4 7.1 %fusion.16 = f32[2,512,256]{2,1,0:T(8,128)S(1)} fusion(bf16[2,512,4096]{2,1,0:T(8,128)(2,1)} %all-gather.4.cloned.1.call-done, bf16[2,256,4096]{2,1,0:T(8,128)(2,1)} %param.15), kind=kOutput, calls=%fused_computation.44 | convolution fusion | flops 2147483648 | bytes 13631488 | tf_op jit(solution)/shard_map/esd,efd->esf/dot_general | solution.py:59
  151.5 1.0 copy-done.7
  152.6 3.3 %fusion = bf16[2,512,256]{2,1,0:T(8,128)(2,1)} fusion(bf16[2,512,4096]{2,1,0:T(8,128)(2,1)S(1)} %copy-done.6, bf16[2,256,4096]{2,1,0:T(8,128)(2,1)S(1)} %copy-done.7, f32[2,512,256]{2,1,0:T(8,128)S(1)} %fusion.16), kind=kOutput, calls=%fused_computation.9 | convolution fusion | flops 2149056512 | bytes 14155776 | tf_op jit(solution)/shard_map/esd,efd->esf/dot_general | solution.py:60
  156.1 0.5 all-gather.8.cloned.1.call-update
  156.6 22.2 %all-gather.6.cloned.1.call-done = bf16[2,512,1024]{2,1,0:T(8,128)(2,1)} async-done(((bf16[2,512,256]{2,1,0:T(8,128)(2,1)}), bf16[2,512,1024]{2,1,0:T(8,128)(2,1)}) %all-gather.6.cloned.1.call-update) | async-done | bytes 2097168 | tf_op jit(solution)/shard_map/all_gather | solution.py:72
  178.8 5.2 %convolution_convert_fusion = bf16[2,512,1024]{2,1,0:T(8,128)(2,1)S(1)} fusion(bf16[2,512,1024]{2,1,0:T(8,128)(2,1)} %all-gather.6.cloned.1.call-done, bf16[2,1024,1024]{2,1,0:T(8,128)(2,1)} %param.17), kind=kOutput, calls=%fused_computation.4 | convolution fusion | flops 2148532224 | bytes 8388608 | tf_op jit(solution)/shard_map/esf,efd->esd/dot_general | solution.py:70
  184.0 3.5 %copy.26 = bf16[2,512,1024]{2,0,1:T(2,128)(2,1)} copy(bf16[2,512,1024]{2,1,0:T(8,128)(2,1)S(1)} %convolution_convert_fusion) | data formatting | bytes 4194304 | tf_op jit(solution)/shard_map/convert_element_type | solution.py:75
  187.5 5.6 %all-to-all-start.1 = ((bf16[2,512,1024]{2,0,1:T(2,128)(2,1)}), bf16[2,512,1024]{2,0,1:T(2,128)(2,1)}, u32[]{:S(2)}, u32[]{:S(2)}) async-start(bf16[2,512,1024]{2,0,1:T(2,128)(2,1)} %copy.26), calls=%async_computation.1 | async-start | bytes 4194304 | tf_op jit(solution)/shard_map/all_to_all | solution.py:76
  193.3 9.7 %all-gather.8.cloned.1.call-done = bf16[256,4096]{1,0:T(8,128)(2,1)} async-done(((bf16[256,1024]{1,0:T(8,128)(2,1)}), bf16[256,4096]{1,0:T(8,128)(2,1)}) %all-gather.8.cloned.1.call-update) | async-done | bytes 2097168 | tf_op jit(solution)/shard_map/all_gather | solution.py:63
  203.0 3.1 %fusion.17 = f32[256,256]{1,0:T(8,128)S(1)} fusion(bf16[256,4096]{1,0:T(8,128)(2,1)} %all-gather.8.cloned.1.call-done, bf16[256,4096]{1,0:T(8,128)(2,1)} %param.18), kind=kOutput, calls=%fused_computation.45 | convolution fusion | flops 536870912 | bytes 4456448 | tf_op jit(solution)/shard_map/td,fd->tf/dot_general | solution.py:66
  206.4 0.7 fusion.1
  207.2 7.6 %all_gather.15 = bf16[256,1024]{1,0:T(8,128)(2,1)} all-gather(bf16[256,256]{1,0:T(8,128)(2,1)S(1)} %fusion.1), channel_id=1, replica_groups=mesh['ep'=8,'tp'=4] {'tp'}, dimensions={1}, use_global_device_ids=true | all-gather | bytes 655360 | tf_op jit(solution)/shard_map/all_gather | solution.py:84
  214.8 27.1 %all-to-all-done.1 = bf16[2,512,1024]{2,0,1:T(2,128)(2,1)} async-done(((bf16[2,512,1024]{2,0,1:T(2,128)(2,1)}), bf16[2,512,1024]{2,0,1:T(2,128)(2,1)}, u32[]{:S(2)}, u32[]{:S(2)}) %all-to-all-start.1) | async-done | bytes 2097184 | tf_op jit(solution)/shard_map/all_to_all | solution.py:76
  241.9 3.5 %copy.27 = bf16[2,8,64,1024]{3,2,0,1:T(8,128)(2,1)} copy(bf16[2,8,64,1024]{3,0,2,1:T(2,128)(2,1)} %bitcast.5) | data formatting | bytes 4194304 | tf_op jit(solution)/shard_map/all_to_all | solution.py:76
  245.4 6.4 %gather_fusion.1 = bf16[768,1024]{1,0:T(8,128)(2,1)} fusion(bf16[1024,1024]{1,0:T(8,128)(2,1)} %bitcast.41, s32[1024]{0:T(1024)S(1)} %pad_clamp_fusion), kind=kCustom, calls=%fused_computation.1 | custom fusion | bytes 3148800 | tf_op jit(solution)/shard_map/gather | solution.py:79
  251.8 5.5 %reshape.77 = f32[256,3,1024]{2,1,0:T(4,128)} reshape(bf16[768,1024]{1,0:T(8,128)(2,1)} %gather_fusion.1) | data formatting | bytes 4718592 | tf_op jit(solution)/shard_map/convert_element_type | solution.py:79
  257.3 4.9 %multiply_reduce_fusion = f32[256,1024]{1,0:T(8,128)S(1)} fusion(f32[256,3,1024]{2,1,0:T(4,128)} %reshape.77, f32[256,3]{1,0:T(8,128)S(1)} %copy.28), kind=kLoop, calls=%fused_computation.3 | loop fusion | flops 1310720 | bytes 4197376 | tf_op jit(solution)/shard_map/reduce_sum | solution.py:80
  262.2 0.8 multiply_reduce_fusion.1
  263.1 5.9 %psum.15 = f32[256]{0:T(256)S(1)} all-reduce(f32[256]{0:T(256)S(1)} %get-tuple-element.5), channel_id=1, replica_groups=mesh['ep'=8,'tp'=4] {'tp'}, use_global_device_ids=true, to_apply=%region_8.9 | all-reduce | flops 256 | bytes 2048 | tf_op jit(solution)/shard_map/psum | solution.py:89
  269.0 1.0 multiply_convert_fusion
  (39 shorter events, 2.1 us)
Async XLA Ops:
  6.5 255.7 %copy-start = (bf16[1024,1024]{1,0:T(8,128)(2,1)S(1)}, bf16[1024,1024]{1,0:T(8,128)(2,1)}, u32[]{:S(2)}) copy-start(bf16[1024,1024]{1,0:T(8,128)(2,1)} %param.20) | copy-start | bytes 6291460
  6.5 137.9 %all-gather.4.cloned.1.call-start = ((), (), s32[]{:S(2)}) async-start(), calls=%async_computation.2 | async-start | bytes 10485760 | tf_op jit(solution)/shard_map/all_gather | solution.py:56
  25.5 5.4 %copy-start.1 = (bf16[256,1024]{1,0:T(8,128)(2,1)}, bf16[256,1024]{1,0:T(8,128)(2,1)S(1)}, u32[]{:S(2)}) copy-start(bf16[256,1024]{1,0:T(8,128)(2,1)S(1)} %fusion.4) | copy-start | bytes 1572868
  86.9 91.9 %all-gather.6.cloned.1.call-start = ((), (), s32[]{:S(2)}) async-start(), calls=%async_computation.3 | async-start | bytes 2621440 | tf_op jit(solution)/shard_map/all_gather | solution.py:72
  144.4 7.1 %copy-start.6 = (bf16[2,512,4096]{2,1,0:T(8,128)(2,1)S(1)}, bf16[2,512,4096]{2,1,0:T(8,128)(2,1)}, u32[]{:S(2)}) copy-start(bf16[2,512,4096]{2,1,0:T(8,128)(2,1)} %all-gather.4.cloned.1.call-done) | copy-start | bytes 25165828
  144.4 8.2 %copy-start.7 = (bf16[2,256,4096]{2,1,0:T(8,128)(2,1)S(1)}, bf16[2,256,4096]{2,1,0:T(8,128)(2,1)}, u32[]{:S(2)}) copy-start(bf16[2,256,4096]{2,1,0:T(8,128)(2,1)} %param.16) | copy-start | bytes 12582916
  155.8 47.1 %all-gather.8.cloned.1.call-start = ((), (), s32[]{:S(2)}) async-start(), calls=%async_computation.4 | async-start | bytes 2621440 | tf_op jit(solution)/shard_map/all_gather | solution.py:63
  187.5 5.6 %copy-start.5 = (f32[256,3]{0,1:T(4,128)S(1)}, f32[256,3]{0,1:T(4,128)}, u32[]{:S(2)}) copy-start(f32[256,3]{0,1:T(4,128)} %param.14) | copy-start | bytes 9220
  187.5 54.4 %all-to-all-start.1 = ((bf16[2,512,1024]{2,0,1:T(2,128)(2,1)}), bf16[2,512,1024]{2,0,1:T(2,128)(2,1)}, u32[]{:S(2)}, u32[]{:S(2)}) async-start(bf16[2,512,1024]{2,0,1:T(2,128)(2,1)} %copy.26), calls=%async_computation.1 | async-start | bytes 4194304 | tf_op jit(solution)/shard_map/all_to_all | solution.py:76
  203.0 3.1 %copy-start.3 = (bf16[256,4096]{1,0:T(8,128)(2,1)S(1)}, bf16[256,4096]{1,0:T(8,128)(2,1)}, u32[]{:S(2)}) copy-start(bf16[256,4096]{1,0:T(8,128)(2,1)} %all-gather.8.cloned.1.call-done) | copy-start | bytes 6291460
  203.0 3.5 %copy-start.8 = (bf16[256,4096]{1,0:T(8,128)(2,1)S(1)}, bf16[256,4096]{1,0:T(8,128)(2,1)}, u32[]{:S(2)}) copy-start(bf16[256,4096]{1,0:T(8,128)(2,1)} %param.19) | copy-start | bytes 6291460
  257.3 4.9 %copy-start.2 = (bf16[256,1024]{1,0:T(8,128)(2,1)S(1)}, bf16[256,1024]{1,0:T(8,128)(2,1)}, u32[]{:S(2)}) copy-start(bf16[256,1024]{1,0:T(8,128)(2,1)} %all_gather.15) | copy-start | bytes 1572868
  262.2 6.8 %copy-start.4 = (f32[1024]{0:T(1024)S(1)}, f32[1024]{0:T(1024)}, u32[]{:S(2)}) copy-start(f32[1024]{0:T(1024)} %param.21) | copy-start | bytes 12292
Sparse Core Ops, SparseCore 0:
  87.0 57.3 all-gather.3
  156.0 22.7 all-gather.5
  180.4 22.5 all-gather.7
where the time goes:
time: 277 us; the launch traced here: 276 us
  waiting for transfers between devices  117 us (42%)
  blocking collectives  74.6 us (27%)
  local copies, waits for them, and re-layouts  32.9 us (12%)
  matrix products  20.2 us (7%)
  between operations  13.3 us (5%)
  other arithmetic  12.7 us (5%)
  starting transfers between devices  5.91 us (2%)
    all_gather x1, waiting for transfers between devices, on_device(): segment = lax.all_gather(arrived, 'tp', axis=2, tiled=True)  57.4 us
    all_to_all x1, blocking collectives, on_device(): lax.all_to_all(outgoing, 'ep', split_axis=0, concat_axis=1, tiled=True)  52.6 us
    all_to_all x1, waiting for transfers between devices, on_device(): lax.all_to_all(expert_out, 'ep', split_axis=1, concat_axis=0, tiled=True)  27.1 us
    all_gather x1, waiting for transfers between devices, on_device(): lax.all_gather(hidden_act, 'tp', axis=2, tiled=True)  22.2 us
    all_gather x1, waiting for transfers between devices, on_device(): segment = lax.all_gather(normed, 'tp', axis=1, tiled=True)  9.71 us
    psum x1, blocking collectives, on_device(): square_sum = lax.psum(jnp.sum(tok_float * tok_float, axis=1), 'tp')  8.4 us
    all_gather x1, blocking collectives, on_device(): lax.all_gather(shared_act, 'tp', axis=1, tiled=True)  7.61 us
    dot_general x1, matrix products, on_device(): jnp.einsum('esd,efd->esf', segment, gate_piece, preferred_element_type=jn...  7.09 us
  transfers between devices with their start and end apart: 4, of which 4 were waited for; matrix products, arithmetic and copies ran while one was open for 5% of the time, Pallas kernels for 0%

commit v1 on v0

v1 whole, which is shorter than its diff:
```python
import functools

import jax
import jax.numpy as jnp
from jax import lax
from jax.experimental import pallas as pl
from jax.experimental.pallas import tpu as pltpu
from jax.sharding import PartitionSpec as P

EPSILON = 1e-06
MESH = pl.DeviceIdType.MESH
GROUPS = 4
CHUNKS = 8


def step_order(n_ep):
    half = n_ep // 2
    far = [half + (half // 2 + k) % half for k in range(half)]
    near = list(range(2, half))
    order = [0, 1]
    while far or near:
        if far:
            order.append(far.pop(0))
        if near:
            order.append(near.pop(0))
    return order


def xor(i, d):
    out = i
    bit = 1
    while bit <= d:
        if d & bit:
            out = out + bit * (1 - 2 * ((i // bit) % 2))
        bit *= 2
    return out


def dot_t(a, b):
    return lax.dot_general(a, b, (((1,), (1,)), ((), ())), preferred_element_type=jnp.float32)


def dot(a, b):
    return jnp.dot(a, b, preferred_element_type=jnp.float32)


def act(gate, up):
    return (gate / (1.0 + jnp.exp(-gate)) * up).astype(jnp.bfloat16)


class Gather:
    def __init__(self, place, source, at, sems, number):
        i, y, c, n_y = place
        ys, yr, ps, pr = sems
        own = y * 2 + c
        partner = (i, y * 2 + (1 - c))
        self.far, self.near = [], []

        def copy(src, dst, s, r, dev):
            return pltpu.make_async_remote_copy(
                src_ref=src, dst_ref=dst, send_sem=s, recv_sem=r, device_id=dev, device_id_type=MESH
            )

        for k in range(1, n_y):
            dev = (i, lax.rem(y + k, n_y) * 2 + c)
            n = number * (n_y - 1) + k - 1
            self.far.append(copy(source, at(own), ys.at[n], yr.at[n], dev))
        self.near.append(copy(source, at(own), ps.at[number * n_y], pr.at[number * n_y], partner))
        for k in range(1, n_y):
            held = at(lax.rem(y + n_y - k, n_y) * 2 + c)
            n = number * n_y + k
            self.near.append(copy(held, held, ps.at[n], pr.at[n], partner))

    def start(self):
        for copy in self.far:
            copy.start()
        self.near[0].start()

    def relay(self):
        for k, copy in enumerate(self.far):
            copy.wait_recv()
            self.near[k + 1].start()

    def finish(self):
        for copy in self.near:
            copy.wait_recv()

    def drain(self):
        for copy in self.far + self.near:
            copy.wait_send()


def kernel(
    n_ep, n_tp, out_ref, norm_ref, whi_ref, wlo_ref, g_hbm, u_hbm, d_hbm, sg_hbm, su_hbm, sd_hbm,
    res_ref,
    seg, sseg, hid, shid, oexp, ret, gw, uw, dw, sgw, suw, sdw,
    wsem, lsem, ds, dr, rs, rr, fys, fyr, fps, fpr, hys, hyr, hps, hpr, sys_, syr, sps, spr,
):
    i, t = lax.axis_index("ep"), lax.axis_index("tp")
    n_y = n_tp // 2
    y, c = t // 2, lax.rem(t, 2)
    place = (i, y, c, n_y)
    own = y * 2 + c
    order = step_order(n_ep)
    _, exp_dev, cap, feat = out_ref.shape
    hidden = gw.shape[1]
    s_hidden = sgw.shape[0]

    loads = [
        pltpu.make_async_copy(a, b, wsem.at[k])
        for k, (a, b) in enumerate(
            ((sg_hbm, sgw), (su_hbm, suw), (g_hbm, gw), (u_hbm, uw), (d_hbm, dw), (sd_hbm, sdw))
        )
    ]
    for load in loads:
        load.start()

    barrier = pltpu.get_barrier_semaphore()
    peers = [(xor(i, d), t) for d in order[1:]]
    peers += [(i, lax.rem(y + k, n_y) * 2 + c) for k in range(1, n_y)]
    peers += [(i, y * 2 + (1 - c))]
    for dev in peers:
        pl.semaphore_signal(barrier, inc=1, device_id=dev, device_id_type=MESH)
    pl.semaphore_wait(barrier, len(peers))

    sends = [None]
    for q in range(1, n_ep):
        sends.append(
            pltpu.make_async_remote_copy(
                src_ref=out_ref.at[q], dst_ref=seg.at[own, :, pl.ds(q * cap, cap), :],
                send_sem=ds.at[q], recv_sem=dr.at[q], device_id=(xor(i, order[q]), t),
                device_id_type=MESH,
            )
        )
    shared = Gather(place, norm_ref, lambda k: sseg.at[k], (sys_, syr, sps, spr), 0)
    for q in range(1, n_ep):
        sends[q].start()
    shared.start()
    stay = pltpu.make_async_copy(out_ref.at[0], seg.at[own, :, pl.ds(0, cap), :], lsem.at[0])
    stay_shared = pltpu.make_async_copy(norm_ref, sseg.at[own], lsem.at[1])
    stay.start()
    stay_shared.start()
    stay.wait()

    per_chunk = n_ep // CHUNKS
    chunk_rows = per_chunk * cap
    rows = n_ep * cap // GROUPS
    chunks = []
    for k in range(CHUNKS):
        at = functools.partial(
            lambda k, j: seg.at[j, :, pl.ds(k * chunk_rows, chunk_rows), :], k
        )
        chunks.append(Gather(place, at(own), at, (fys, fyr, fps, fpr), k))
    acts = []
    for g in range(GROUPS):
        at = functools.partial(lambda g, j: hid.at[j, :, pl.ds(g * rows, rows), :], g)
        acts.append(Gather(place, at(own), at, (hys, hyr, hps, hpr), g))
    shared_act = Gather(place, shid.at[own], lambda k: shid.at[k], (sys_, syr, sps, spr), 1)

    def begin(k):
        for q in range(k * per_chunk, (k + 1) * per_chunk):
            if q:
                sends[q].wait_recv()
        chunks[k].start()

    def gate_up(g):
        for k in range(g * CHUNKS // GROUPS, (g + 1) * CHUNKS // GROUPS):
            chunks[k].finish()
        part = pl.ds(g * rows, rows)

        @pl.loop(0, exp_dev)
        def _(e):
            gate = up = None
            for k in range(n_tp):
                x = seg[k, e, part, :]
                a = dot_t(x, gw[e, :, k * feat:(k + 1) * feat])
                b = dot_t(x, uw[e, :, k * feat:(k + 1) * feat])
                gate = a if gate is None else gate + a
                up = b if up is None else up + b
            hid[own, e, part, :] = act(gate, up)

        acts[g].start()

    per_group = n_ep // GROUPS
    returns = []

    def down(g):
        acts[g].relay()
        acts[g].finish()
        part = pl.ds(g * rows, rows)

        @pl.loop(0, exp_dev)
        def _(e):
            total = None
            for k in range(n_tp):
                a = dot(hid[k, e, part, :], dw[e, k * hidden:(k + 1) * hidden, :])
                total = a if total is None else total + a
            oexp[e, part, :] = total.astype(jnp.bfloat16)

        for q in range(g * per_group, (g + 1) * per_group):
            src = oexp.at[:, pl.ds(q * cap, cap), :]
            if q == 0:
                copy = pltpu.make_async_copy(src, ret.at[0], lsem.at[0])
            else:
                copy = pltpu.make_async_remote_copy(
                    src_ref=src, dst_ref=ret.at[q], send_sem=rs.at[q], recv_sem=rr.at[q],
                    device_id=(xor(i, order[q]), t), device_id_type=MESH,
                )
            copy.start()
            returns.append(copy)

    begin(0)
    begin(1)
    shared.relay()
    chunks[0].relay()
    stay_shared.wait()
    shared.finish()
    loads[0].wait()
    loads[1].wait()
    gate = up = None
    for k in range(n_tp):
        x = sseg[k]
        a = dot_t(x, sgw[:, k * feat:(k + 1) * feat])
        b = dot_t(x, suw[:, k * feat:(k + 1) * feat])
        gate = a if gate is None else gate + a
        up = b if up is None else up + b
    shid[own] = act(gate, up)
    shared_act.start()
    loads[2].wait()
    loads[3].wait()
    loads[4].wait()
    loads[5].wait()
    span = CHUNKS // GROUPS
    for k in range(2, CHUNKS):
        begin(k)
        chunks[k - 1].relay()
        if k % span == span - 1:
            g = k // span - 1
            gate_up(g)
            if g:
                down(g - 1)
    chunks[CHUNKS - 1].relay()
    gate_up(GROUPS - 1)
    down(GROUPS - 2)
    shared_act.relay()
    down(GROUPS - 1)
    shared_act.finish()
    total = None
    for k in range(n_tp):
        a = dot(shid[k], sdw[k * s_hidden:(k + 1) * s_hidden, :])
        total = a if total is None else total + a
    res_ref[...] = total
    width = per_group * exp_dev * cap
    for g in range(GROUPS):
        for q in range(g * per_group, (g + 1) * per_group):
            if q:
                returns[q].wait_recv()
            else:
                returns[q].wait()
        piece = ret[g * per_group:(g + 1) * per_group].reshape(width, feat)
        cols = pl.ds(g * width, width)
        res_ref[...] += dot(whi_ref[:, cols], piece) + dot(wlo_ref[:, cols], piece)
    for q in range(1, n_ep):
        sends[q].wait_send()
        returns[q].wait_send()
    for gather in chunks + acts + [shared, shared_act]:
        gather.drain()


def exchange(n_ep, n_tp, outgoing, normed, whi, wlo, gate, up, down, s_gate, s_up, s_down):
    exp_dev, hidden, width = gate.shape
    _, _, cap, feat = outgoing.shape
    tok = normed.shape[0]
    s_hidden = s_gate.shape[0]
    n_y = n_tp // 2
    bf = jnp.bfloat16
    dma = pltpu.SemaphoreType.DMA
    far, near = n_y - 1, n_y
    vmem, hbm = pl.BlockSpec(memory_space=pltpu.VMEM), pl.BlockSpec(memory_space=pl.ANY)
    return pl.pallas_call(
        functools.partial(kernel, n_ep, n_tp),
        out_shape=jax.ShapeDtypeStruct((tok, feat), jnp.float32),
        in_specs=[vmem] * 4 + [hbm] * 6,
        out_specs=vmem,
        scratch_shapes=[
            pltpu.VMEM((n_tp, exp_dev, n_ep * cap, feat), bf),
            pltpu.VMEM((n_tp, tok, feat), bf),
            pltpu.VMEM((n_tp, exp_dev, n_ep * cap, hidden), bf),
            pltpu.VMEM((n_tp, tok, s_hidden), bf),
            pltpu.VMEM((exp_dev, n_ep * cap, feat), bf),
            pltpu.VMEM((n_ep, exp_dev, cap, feat), bf),
            pltpu.VMEM(gate.shape, bf),
            pltpu.VMEM(up.shape, bf),
            pltpu.VMEM(down.shape, bf),
            pltpu.VMEM(s_gate.shape, bf),
            pltpu.VMEM(s_up.shape, bf),
            pltpu.VMEM(s_down.shape, bf),
            dma((6,)), dma((2,)),
            dma((n_ep,)), dma((n_ep,)), dma((n_ep,)), dma((n_ep,)),
            dma((CHUNKS * far,)), dma((CHUNKS * far,)), dma((CHUNKS * near,)), dma((CHUNKS * near,)),
            dma((GROUPS * far,)), dma((GROUPS * far,)), dma((GROUPS * near,)), dma((GROUPS * near,)),
            dma((2 * far,)), dma((2 * far,)), dma((2 * near,)), dma((2 * near,)),
        ],
        compiler_params=pltpu.CompilerParams(
            collective_id=0, has_side_effects=True, vmem_limit_bytes=56 * 1024 * 1024
        ),
    )(outgoing, normed, whi, wlo, gate, up, down, s_gate, s_up, s_down)


def on_device(
    n_ep, n_tp, tokens, pre_gain, expert_ids, route_weight, expert_gate, expert_up, expert_down,
    shared_gate, shared_up, shared_down, out_gain,
):
    tok_count, top_count = expert_ids.shape
    exp_dev = expert_gate.shape[0]
    width = expert_gate.shape[2]
    experts = exp_dev * n_ep
    capacity = 4 * tok_count * top_count // (3 * experts)
    feat = tokens.shape[1]
    tok_float = tokens.astype(jnp.float32)
    square_sum = lax.psum(jnp.sum(tok_float * tok_float, axis=1), "tp")
    normed = (tok_float * lax.rsqrt(square_sum[:, None] / width + EPSILON) * pre_gain).astype(
        jnp.bfloat16
    )
    i = lax.axis_index("ep")
    steps = jnp.array(step_order(n_ep), jnp.int32)
    names = ((i ^ steps)[:, None] * exp_dev + jnp.arange(exp_dev, dtype=jnp.int32)).reshape(experts)
    same = expert_ids[:, :, None] == names[None, None, :]
    member = jnp.any(same, axis=1)
    weight = jnp.sum(jnp.where(same, route_weight[:, :, None], 0.0), axis=1)
    row = jnp.arange(tok_count, dtype=jnp.int32)
    earlier = (row[None, :] < row[:, None]).astype(jnp.bfloat16)
    before = jnp.dot(earlier, member.astype(jnp.bfloat16), preferred_element_type=jnp.float32)
    slot = jnp.where(member, before.astype(jnp.int32), -1)
    places = jnp.arange(capacity, dtype=jnp.int32)
    pick = (slot.T[:, None, :] == places[None, :, None]).astype(jnp.bfloat16)
    outgoing = jnp.dot(
        pick.reshape(experts * capacity, tok_count), normed, preferred_element_type=jnp.float32
    ).astype(jnp.bfloat16)
    outgoing = outgoing.reshape(n_ep, exp_dev, capacity, feat)
    high = lax.reduce_precision(weight, 8, 7)
    low = weight - high
    here = slot[:, :, None] == places[None, None, :]

    def spread(values):
        return jnp.where(here, values[:, :, None], 0.0).astype(jnp.bfloat16).reshape(
            tok_count, experts * capacity
        )

    summed = exchange(
        n_ep, n_tp, outgoing, normed, spread(high), spread(low), expert_gate, expert_up,
        expert_down, shared_gate, shared_up, shared_down,
    )
    out_square = lax.psum(jnp.sum(summed * summed, axis=1), "tp")
    return (summed * lax.rsqrt(out_square[:, None] / width + EPSILON) * out_gain).astype(
        jnp.bfloat16
    )


def solution(mesh):
    return jax.shard_map(
        functools.partial(on_device, mesh.shape["ep"], mesh.shape["tp"]),
        mesh=mesh,
        in_specs=(
            P("ep", "tp"),
            P("tp"),
            P("ep", None),
            P("ep", None),
            P("ep", "tp", None),
            P("ep", "tp", None),
            P("ep", None, "tp"),
            P("tp", None),
            P("tp", None),
            P(None, "tp"),
            P("tp"),
        ),
        out_specs=P("ep", "tp"),
        check_vma=False,
    )
```

time: 277 us -> 153 us (0.55)
  Pallas kernels: 0 us -> 123 us
  waiting for transfers between devices: 117 us -> 0 us
  blocking collectives: 74.6 us -> 14.4 us
  local copies, waits for them, and re-layouts: 32.9 us -> 1.89 us
  matrix products: 20.2 us -> 2.23 us
  between operations: 13.3 us -> 0.1 us
  starting transfers between devices: 5.91 us -> 0 us
    pallas_call x0 -> x1, Pallas kernels: none -> 123 us  [exchange(): pl.pallas_call(functools.partial(kernel, n_ep, n_tp), out_shape=jax.Shape...]
    all_gather x3 -> x0, waiting for transfers between devices: 89.4 us -> none  [the longest x1 57.4 us: on_device(): segment = lax.all_gather(arrived, 'tp', axis=2, tiled=True)]
    all_to_all x1 -> x0, blocking collectives: 52.6 us -> none  [on_device(): lax.all_to_all(outgoing, 'ep', split_axis=0, concat_axis=1, tiled=True)]
    all_to_all x1 -> x0, waiting for transfers between devices: 27.1 us -> none  [on_device(): lax.all_to_all(expert_out, 'ep', split_axis=1, concat_axis=0, tiled=True)]
    dot_general x6 -> x2, matrix products: 20.2 us -> 2.23 us  [the longest x1 2.07 us: on_device(): jnp.dot(pick.reshape(experts * capacity, tok_count), normed, preferred_el...]
    gather x2 -> x0, local copies, waits for them, and re-layouts: 11.8 us -> none  [the longest x1 6.42 us: on_device(): returned[dest_index].reshape(tok_count, top_count, feat_local)]
    convert_element_type x2 -> x0, local copies, waits for them, and re-layouts: 8.96 us -> none  [the longest x1 5.47 us: on_device(): returned[dest_index].reshape(tok_count, top_count, feat_local)]
    all_gather x1 -> x0, blocking collectives: 7.61 us -> none  [on_device(): lax.all_gather(shared_act, 'tp', axis=1, tiled=True)]
  transfers between devices with their start and end apart: 4 -> 0, of which waited for: 4 -> 0; matrix products, arithmetic and copies ran while one was open for 5% -> 0% of each run, Pallas kernels for 0% -> 0%
where the time goes in v1:
time: 153 us; the launch traced here: 152 us
  Pallas kernels  123 us (80%)
  blocking collectives  14.4 us (9%)
  other arithmetic  10.6 us (7%)
  matrix products  2.23 us (1%)
  local copies, waits for them, and re-layouts  1.89 us (1%)
    pallas_call x1, Pallas kernels, exchange(): pl.pallas_call(functools.partial(kernel, n_ep, n_tp), out_shape=jax.Shape...  123 us
    psum x1, blocking collectives, on_device(): square_sum = lax.psum(jnp.sum(tok_float * tok_float, axis=1), 'tp')  8.4 us
    psum x1, blocking collectives, on_device(): out_square = lax.psum(jnp.sum(summed * summed, axis=1), 'tp')  5.98 us

profile of v1, /device:TPU:0, one launch (start us, length us, event | category | flops | bytes accessed | tf_op | source)
XLA Modules:
  0.0 152.5 jit_solution(10728024629115768229)
XLA Ops:
  0.0 0.0 copy-start.1
  0.0 0.0 copy-start.2
  0.0 0.7 xor_multiply_fusion
  0.7 1.2 fusion.1
  1.9 8.4 %psum.14 = f32[256]{0:T(256)S(1)} all-reduce(f32[256]{0:T(256)S(1)} %fusion.1), channel_id=1, replica_groups=mesh['ep'=8,'tp'=4] {'tp'}, use_global_device_ids=true, to_apply=%region_2.0 | all-reduce | flops 256 | bytes 2048 | tf_op jit(solution)/shard_map/psum | solution.py:321
  10.4 0.1 iota_add_fusion
  10.4 0.1 add.35
  10.5 0.8 compare_reduce_fusion
  11.3 0.1 eq.60
  11.4 0.2 fusion
  11.5 0.8 fusion.4
  12.3 0.2 bitcast_compare_fusion
  12.6 0.2 copy.22
  12.8 0.0 copy-done.1
  12.8 0.0 copy-done.2
  12.8 0.2 fusion.3.norm_ref
  13.0 0.0 copy-start
  13.1 1.0 copy.23
  14.1 0.1 eq.63
  14.2 0.3 copy.21
  14.5 2.1 %select_convert_fusion = (bf16[256,1024]{1,0:T(8,128)(2,1)}, pred[256,1024]{1,0:T(8,128)(4,1)S(1)}) fusion(bf16[256,1024]{1,0:T(8,128)(2,1)} %copy.23, s32[256,1024]{1,0:T(8,128)S(1)} %copy.21, s32[1024]{0:T(1024)S(1)} %eq.60), kind=kLoop, calls=%fused_computation.11 | loop fusion | flops 524288 | bytes 2363392 | tf_op jit(solution)/shard_map/convert_element_type | solution.py:346
  16.6 1.0 select_convert_fusion.1.whi_ref
  17.6 0.0 copy-done
  17.6 2.1 %convolution_convert_fusion = bf16[1024,1024]{1,0:T(8,128)(2,1)} fusion(pred[1024,256]{1,0:T(32,128)(4,1)S(1)} %bitcast_compare_fusion, bf16[256,1024]{1,0:T(8,128)(2,1)S(1)} %fusion.3.norm_ref), kind=kOutput, calls=%fused_computation | convolution fusion | flops 537919488 | bytes 2883584 | tf_op jit(solution)/shard_map/dot_general | solution.py:337
  19.6 0.0 copy-start.3
  19.6 123.3 %shard_map.118 = f32[256,1024]{1,0:T(8,128)} custom-call(bf16[8,2,64,1024]{3,2,1,0:T(8,128)(2,1)} %bitcast.10, bf16[256,1024]{1,0:T(8,128)(2,1)} %copy-done, bf16[256,1024]{1,0:T(8,128)(2,1)} %select_convert_fusion.1.whi_ref, bf16[256,1024]{1,0:T(8,128)(2,1)} %get-tuple-element.5.wlo_ref, bf16[2,256,4096]{2,1,0:T(8,128)(2,1)} %g_hbm.1, ...), custom_call_target="tpu_custom_call" | custom-call | tf_op jit(solution)/shard_map/pallas_call | solution.py:280
  142.9 1.4 multiply_reduce_fusion
  144.3 6.0 %psum.15 = f32[256]{0:T(256)S(1)} all-reduce(f32[256]{0:T(256)S(1)} %multiply_reduce_fusion), channel_id=1, replica_groups=mesh['ep'=8,'tp'=4] {'tp'}, use_global_device_ids=true, to_apply=%region_5.6 | all-reduce | flops 256 | bytes 2048 | tf_op jit(solution)/shard_map/psum | solution.py:354
  150.3 0.0 copy-done.3
  150.3 2.2 %multiply_convert_fusion = bf16[256,1024]{1,0:T(8,128)(2,1)} fusion(f32[256,1024]{1,0:T(8,128)} %shard_map.118, f32[1024]{0:T(1024)S(1)} %copy-done.3, f32[256]{0:T(256)S(1)} %add_rsqrt_fusion), kind=kLoop, calls=%fused_computation.9 | loop fusion | flops 786432 | bytes 1577984 | tf_op jit(solution)/shard_map/convert_element_type | solution.py:355
  (6 shorter events, 0.1 us)
Async XLA Ops:
  0.0 12.8 %copy-start.1 = (bf16[256,1024]{1,0:T(8,128)(2,1)S(1)}, bf16[256,1024]{1,0:T(8,128)(2,1)}, u32[]{:S(2)}) copy-start(bf16[256,1024]{1,0:T(8,128)(2,1)} %param.12) | copy-start | bytes 1572868
  0.0 12.8 %copy-start.2 = (f32[1024]{0:T(1024)S(1)}, f32[1024]{0:T(1024)}, u32[]{:S(2)}) copy-start(f32[1024]{0:T(1024)} %param.13) | copy-start | bytes 12292
  13.0 4.5 %copy-start = (bf16[256,1024]{1,0:T(8,128)(2,1)}, bf16[256,1024]{1,0:T(8,128)(2,1)S(1)}, u32[]{:S(2)}) copy-start(bf16[256,1024]{1,0:T(8,128)(2,1)S(1)} %fusion.3.norm_ref) | copy-start | bytes 1572868
  19.6 130.6 %copy-start.3 = (f32[1024]{0:T(1024)S(1)}, f32[1024]{0:T(1024)}, u32[]{:S(2)}) copy-start(f32[1024]{0:T(1024)} %param.22) | copy-start | bytes 12292

commit v2 on v1

--- a/solution.py
+++ b/solution.py
@@ -16,14 +16,7 @@
 def step_order(n_ep):
     half = n_ep // 2
     far = [half + (half // 2 + k) % half for k in range(half)]
-    near = list(range(2, half))
-    order = [0, 1]
-    while far or near:
-        if far:
-            order.append(far.pop(0))
-        if near:
-            order.append(near.pop(0))
-    return order
+    return [0, 1] + far + list(range(2, half))
 
 
 def xor(i, d):
@@ -157,6 +150,8 @@
         acts.append(Gather(place, at(own), at, (hys, hyr, hps, hpr), g))
     shared_act = Gather(place, shid.at[own], lambda k: shid.at[k], (sys_, syr, sps, spr), 1)
 
+    span = CHUNKS // GROUPS
+
     def begin(k):
         for q in range(k * per_chunk, (k + 1) * per_chunk):
             if q:
@@ -209,8 +204,8 @@
             copy.start()
             returns.append(copy)
 
-    begin(0)
-    begin(1)
+    for k in range(span):
+        begin(k)
     shared.relay()
     chunks[0].relay()
     stay_shared.wait()
@@ -228,22 +223,28 @@
     shared_act.start()
     loads[2].wait()
     loads[3].wait()
+    for k in range(1, span):
+        chunks[k].relay()
+    gate_up(0)
     loads[4].wait()
     loads[5].wait()
-    span = CHUNKS // GROUPS
-    for k in range(2, CHUNKS):
+    for k in range(span, 2 * span):
         begin(k)
-        chunks[k - 1].relay()
-        if k % span == span - 1:
-            g = k // span - 1
-            gate_up(g)
-            if g:
-                down(g - 1)
-    chunks[CHUNKS - 1].relay()
-    gate_up(GROUPS - 1)
-    down(GROUPS - 2)
+        chunks[k - 1].relay() if k > span else None
+    down(0)
     shared_act.relay()
-    down(GROUPS - 1)
+    for g in range(1, GROUPS):
+        last = (g + 1) * span - 1
+        chunks[last].relay()
+        gate_up(g)
+        ahead = list(range(last + 1, min(last + 1 + span, CHUNKS)))
+        for k in ahead[:1] if g == 1 else ahead:
+            begin(k)
+        down(g)
+        for k in ahead[1:] if g == 1 else ():
+            begin(k)
+        for k in ahead[:-1]:
+            chunks[k].relay()
     shared_act.finish()
     total = None
     for k in range(n_tp):
@@ -307,6 +308,10 @@
     )(outgoing, normed, whi, wlo, gate, up, down, s_gate, s_up, s_down)
 
 
+def total_over_tp(values):
+    return jnp.sum(lax.all_gather(values, "tp"), axis=0)
+
+
 def on_device(
     n_ep, n_tp, tokens, pre_gain, expert_ids, route_weight, expert_gate, expert_up, expert_down,
     shared_gate, shared_up, shared_down, out_gain,
@@ -318,7 +323,7 @@
     capacity = 4 * tok_count * top_count // (3 * experts)
     feat = tokens.shape[1]
     tok_float = tokens.astype(jnp.float32)
-    square_sum = lax.psum(jnp.sum(tok_float * tok_float, axis=1), "tp")
+    square_sum = total_over_tp(jnp.sum(tok_float * tok_float, axis=1))
     normed = (tok_float * lax.rsqrt(square_sum[:, None] / width + EPSILON) * pre_gain).astype(
         jnp.bfloat16
     )
@@ -351,7 +356,7 @@
         n_ep, n_tp, outgoing, normed, spread(high), spread(low), expert_gate, expert_up,
         expert_down, shared_gate, shared_up, shared_down,
     )
-    out_square = lax.psum(jnp.sum(summed * summed, axis=1), "tp")
+    out_square = total_over_tp(jnp.sum(summed * summed, axis=1))
     return (summed * lax.rsqrt(out_square[:, None] / width + EPSILON) * out_gain).astype(
         jnp.bfloat16
     )

time: 153 us -> 150 us (0.980)
  blocking collectives: 14.4 us -> 11.1 us
    psum x2 -> x0, blocking collectives: 14.4 us -> none  [the longest x1 8.4 us: on_device(): square_sum = lax.psum(jnp.sum(tok_float * tok_float, axis=1), 'tp')]
    all_gather x0 -> x2, blocking collectives: none -> 11.1 us  [total_over_tp(): return jnp.sum(lax.all_gather(values, 'tp'), axis=0)]
where the time goes in v2:
time: 150 us
  Pallas kernels  124 us (83%)
  blocking collectives  11.1 us (7%)
  other arithmetic  10.6 us (7%)
  matrix products  2.22 us (1%)
  local copies, waits for them, and re-layouts  1.89 us (1%)
    pallas_call x1, Pallas kernels, exchange(): pl.pallas_call(functools.partial(kernel, n_ep, n_tp), out_shape=jax.Shape...  124 us
    all_gather x2, blocking collectives, total_over_tp(): return jnp.sum(lax.all_gather(values, 'tp'), axis=0)  11.1 us
    convert_element_type x2, other arithmetic, spread(): jnp.where(here, values[:, :, None], 0.0).astype(jnp.bfloat16)  3.04 us

profile of v2, /device:TPU:0, one launch (start us, length us, event | category | flops | bytes accessed | tf_op | source)
XLA Modules:
  0.0 149.6 jit_solution(8232249818115344750)
XLA Ops:
  0.0 0.0 copy-start.1
  0.0 0.0 copy-start.2
  0.0 0.7 xor_multiply_fusion
  0.7 1.2 fusion.1
  1.9 6.0 %all-gather.2 = f32[4,1,256]{2,1,0:T(1,128)S(1)} all-gather(f32[1,1,256]{2,1,0:T(1,128)S(1)} %bitcast.17), channel_id=2, replica_groups=mesh['ep'=8,'tp'=4] {'tp'}, dimensions={0}, use_global_device_ids=true | all-gather | bytes 5120 | tf_op jit(solution)/shard_map/all_gather | solution.py:312
  8.0 0.1 iota_add_fusion
  8.1 0.1 add.39
  8.2 0.8 compare_reduce_fusion
  8.9 0.1 eq.60
  9.0 0.2 fusion
  9.2 0.8 fusion.4
  10.0 0.2 bitcast_compare_fusion
  10.3 0.2 copy.27
  10.5 0.0 copy-done.1
  10.5 0.0 copy-done.2
  10.5 0.2 fusion.3.norm_ref
  10.7 0.0 copy-start
  10.8 1.0 copy.28
  11.8 0.1 eq.63
  11.9 0.3 copy.26
  12.2 2.1 %select_convert_fusion = (bf16[256,1024]{1,0:T(8,128)(2,1)}, pred[256,1024]{1,0:T(8,128)(4,1)S(1)}) fusion(bf16[256,1024]{1,0:T(8,128)(2,1)} %copy.28, s32[256,1024]{1,0:T(8,128)S(1)} %copy.26, s32[1024]{0:T(1024)S(1)} %eq.60), kind=kLoop, calls=%fused_computation.11 | loop fusion | flops 524288 | bytes 2363392 | tf_op jit(solution)/shard_map/convert_element_type | solution.py:351
  14.3 1.0 select_convert_fusion.1.whi_ref
  15.2 0.0 copy-done
  15.2 2.1 %convolution_convert_fusion = bf16[1024,1024]{1,0:T(8,128)(2,1)} fusion(pred[1024,256]{1,0:T(32,128)(4,1)S(1)} %bitcast_compare_fusion, bf16[256,1024]{1,0:T(8,128)(2,1)S(1)} %fusion.3.norm_ref), kind=kOutput, calls=%fused_computation | convolution fusion | flops 537919488 | bytes 2883584 | tf_op jit(solution)/shard_map/dot_general | solution.py:342
  17.3 0.0 copy-start.3
  17.3 123.6 %shard_map.118 = f32[256,1024]{1,0:T(8,128)} custom-call(bf16[8,2,64,1024]{3,2,1,0:T(8,128)(2,1)} %bitcast.12, bf16[256,1024]{1,0:T(8,128)(2,1)} %copy-done, bf16[256,1024]{1,0:T(8,128)(2,1)} %select_convert_fusion.1.whi_ref, bf16[256,1024]{1,0:T(8,128)(2,1)} %get-tuple-element.5.wlo_ref, bf16[2,256,4096]{2,1,0:T(8,128)(2,1)} %g_hbm.1, ...), custom_call_target="tpu_custom_call" | custom-call | tf_op jit(solution)/shard_map/pallas_call | solution.py:281
  140.9 1.4 multiply_reduce_fusion
  142.3 5.1 %all-gather.3 = f32[4,1,256]{2,1,0:T(1,128)S(1)} all-gather(f32[1,1,256]{2,1,0:T(1,128)S(1)} %bitcast.18), channel_id=3, replica_groups=mesh['ep'=8,'tp'=4] {'tp'}, dimensions={0}, use_global_device_ids=true | all-gather | bytes 5120 | tf_op jit(solution)/shard_map/all_gather | solution.py:312
  147.4 0.0 copy-done.3
  147.4 2.2 %multiply_convert_fusion = bf16[256,1024]{1,0:T(8,128)(2,1)} fusion(f32[256,1024]{1,0:T(8,128)} %shard_map.118, f32[1024]{0:T(1024)S(1)} %copy-done.3, f32[256]{0:T(256)S(1)} %add_rsqrt_fusion), kind=kLoop, calls=%fused_computation.9 | loop fusion | flops 786432 | bytes 1577984 | tf_op jit(solution)/shard_map/convert_element_type | solution.py:360
  (8 shorter events, 0.2 us)
Async XLA Ops:
  0.0 10.5 %copy-start.1 = (bf16[256,1024]{1,0:T(8,128)(2,1)S(1)}, bf16[256,1024]{1,0:T(8,128)(2,1)}, u32[]{:S(2)}) copy-start(bf16[256,1024]{1,0:T(8,128)(2,1)} %param.12) | copy-start | bytes 1572868
  0.0 10.5 %copy-start.2 = (f32[1024]{0:T(1024)S(1)}, f32[1024]{0:T(1024)}, u32[]{:S(2)}) copy-start(f32[1024]{0:T(1024)} %param.13) | copy-start | bytes 12292
  10.7 4.5 %copy-start = (bf16[256,1024]{1,0:T(8,128)(2,1)}, bf16[256,1024]{1,0:T(8,128)(2,1)S(1)}, u32[]{:S(2)}) copy-start(bf16[256,1024]{1,0:T(8,128)(2,1)S(1)} %fusion.3.norm_ref) | copy-start | bytes 1572868
  17.3 130.1 %copy-start.3 = (f32[1024]{0:T(1024)S(1)}, f32[1024]{0:T(1024)}, u32[]{:S(2)}) copy-start(f32[1024]{0:T(1024)} %param.22) | copy-start | bytes 12292
